TPU v7x, 256 devices: a whole 4x4x8 slice. The times are simulated.
256 devices in a mesh: ep: 64 (over z, y, core), tp: 4 (over x).
Axes of the slice: x: 4, y: 4, z: 8, core: 2. Of those that a mesh axis runs over, the one named last changes fastest.
Arguments:
- tokens: bfloat16 [16384, 1024], P('ep'), may hold values from -6 to 6
- cotangent: bfloat16 [16384, 1024], P('ep'), may hold values from -1.5 to 1.5
- routing: int32 [16384, 2], P('ep'), may hold values from 0 to 127, all different within a row; in each aligned block of 256 rows (0 to 255, 256 to 511, ...) at most 12 rows name the same one
- gate_weights: float32 [16384, 2], P('ep'), may hold values from 0.1 to 0.9
- gate_proj: bfloat16 [128, 1024, 512], P('ep', None, 'tp'), may hold values from -0.1875 to 0.1875
- up_proj: bfloat16 [128, 1024, 512], P('ep', None, 'tp'), may hold values from -0.1875 to 0.1875
- down_proj: bfloat16 [128, 512, 1024], P('ep', 'tp'), may hold values from -0.25 to 0.25
Outputs:
- tokens_grad: bfloat16 [16384, 1024], P('ep')
- gates_grad: float32 [16384, 2], P('ep')
- gate_proj_grad: float32 [128, 1024, 512], P('ep', None, 'tp')
- up_proj_grad: float32 [128, 1024, 512], P('ep', None, 'tp')
- down_proj_grad: float32 [128, 512, 1024], P('ep', 'tp')
Inputs may be any that keep to these rules, and one draw needn't show every extreme that they name: `routing`: each row names 2 different experts; every expert is named by some row; within each aligned block of 256 rows (the tokens of one index of ep) no expert is named by more than 12 rows, a bound that some block reaches.
All inputs are finite; a program needn't handle non-finite values.
Results may differ from a plain program's by a relative error of at most 0.0015.
Values may be sent and summed in bfloat16 or wider, within the bound.
No kernel may reach another device: no remote copies, remote signals or barrier semaphores. Data moves between devices by JAX's collectives and lax.ppermute only.
A program may use at most 128 MiB of HBM per device.

v0:
```python
import jax
import jax.numpy as jnp
from jax import lax
from jax.experimental import pallas as pl
from jax.experimental.pallas import tpu as pltpu
from jax.sharding import PartitionSpec as P


F32 = jnp.float32
I16 = jnp.int16
BF16 = jnp.bfloat16
I32 = jnp.int32
LANES = 128
SUBLANES = 8
BLOCK = 16
HALVES = 2
TOP_CODE = 32766.0
STEPS = 8192.0
FINE = 32768.0
VMEM = pltpu.VMEM
SMEM = pltpu.SMEM
NN = ((1,), (0,))
NT = ((1,), (1,))
TN = ((0,), (0,))


def mm(a, b, dims=NN):
    return lax.dot_general(a, b, (dims, ((), ())), preferred_element_type=F32)


def iota(shape, dim):
    return lax.broadcasted_iota(I32, shape, dim)


def split3(value):
    high = value.astype(BF16)
    rest = value - high.astype(F32)
    middle = rest.astype(BF16)
    low = (rest - middle.astype(F32)).astype(BF16)
    return high, middle, low


def exponent(value):
    return jnp.floor(jnp.log(jnp.maximum(value, 1e-30)) * 1.4426950408889634)


def row_scale(power, steps):
    return steps * jnp.exp2(power) * (1.0 / (STEPS * TOP_CODE))


def code_rows(value):
    largest = jnp.maximum(jnp.max(jnp.abs(value), axis=1, keepdims=True), 1e-30)
    power = exponent(largest)
    steps = jnp.ceil(largest * jnp.exp2(-power) * STEPS)
    return jnp.round(value * (1.0 / row_scale(power, steps))), power, steps


def code_values(value):
    power = exponent(jnp.abs(value))
    value = value * jnp.exp2(-power) * STEPS
    coarse = jnp.round(value)
    return power, coarse, jnp.round((value - coarse) * FINE)


def decode_values(power, coarse, fine):
    return (coarse + fine * (1.0 / FINE)) * (jnp.exp2(power) * (1.0 / STEPS))


def to_code(value):
    return value.astype(I32).astype(I16)


def from_code(value):
    return value.astype(I32).astype(F32)


def dispatch_kernel(
    experts, local_experts, quarter, member, routing, weights, tokens, cotangent, rows_out, pick, laid
):
    token_count, _ = tokens.shape
    slots = pick.shape[1]
    group = local_experts * quarter
    devices = experts // local_experts
    expert = iota((experts, token_count), 0)
    chosen = [routing[k : k + 1, :] for k in range(2)]
    onehot = [jnp.where(expert == c, 1.0, 0.0) for c in chosen]
    earlier = iota((token_count, token_count), 0)
    later = iota((token_count, token_count), 1)
    upper = jnp.where(earlier < later, 1.0, 0.0).astype(BF16)
    before = mm((onehot[0] + onehot[1]).astype(BF16), upper)
    slot = iota((slots, token_count), 0)
    hits = []
    for k in range(2):
        position = jnp.sum(onehot[k] * before, axis=0, keepdims=True).astype(I32)
        local = position - member[0] * quarter
        present = (local >= 0) & (local < quarter)
        device = chosen[k] // local_experts
        within = (chosen[k] - device * local_experts) * quarter + local
        hits.append(slot == jnp.where(present, within * devices + device, -1))
        pick[k] = jnp.where(hits[k], 1.0, 0.0).astype(BF16)
    weighted = jnp.where(hits[0], weights[0:1, :], jnp.where(hits[1], weights[1:2, :], 0.0))
    slot_weight = jnp.sum(weighted, axis=1, keepdims=True)
    both = jnp.where(hits[0] | hits[1], 1.0, 0.0).astype(BF16)
    values = (mm(both, tokens[...]), mm(both, cotangent[...]) * slot_weight)
    tiles = laid.shape[0]
    chunk = HALVES * 2 * group
    for kind, value in enumerate(values):
        for h in range(HALVES):
            for at in range(group):
                to = (2 * h + kind) * group + at
                for tile in range(tiles):
                    column = (h * tiles + tile) * LANES
                    piece = value[at * devices : (at + 1) * devices, column : column + LANES]
                    laid[tile, pl.ds(to, devices, stride=chunk), :] = piece
    for tile in range(tiles):
        rows_out[:, tile * LANES : (tile + 1) * LANES] = laid[tile].astype(BF16)


def land(source, expert, local_experts, quarter, rows, scaled, offset):
    half = source.shape[1]
    group = local_experts * quarter
    chunk = HALVES * 2 * group
    out_rows = BLOCK * quarter
    index = iota((HALVES * 2 * out_rows, 1), 0)
    kind = index // out_rows
    rest = index - kind * out_rows
    slot = rest // BLOCK
    wanted = (rest - slot * BLOCK) * chunk + kind * group + expert * quarter + slot
    column = iota((HALVES * 2 * out_rows, BLOCK * chunk), 1)
    permutation = jnp.where(column == wanted, 1.0, 0.0).astype(BF16)
    for block in range(source.shape[0] // (BLOCK * chunk)):
        moved = mm(permutation, source[block * BLOCK * chunk : (block + 1) * BLOCK * chunk, :])
        moved = moved.astype(BF16)
        at = slice(offset + block * out_rows, offset + (block + 1) * out_rows)
        for h in range(HALVES):
            columns = slice(h * half, (h + 1) * half)
            first = 2 * h * out_rows
            rows[at, columns] = moved[first : first + out_rows]
            scaled[at, columns] = moved[first + out_rows : first + 2 * out_rows]


def hidden_terms(gate_pre, up_pre, hidden_grad):
    gate_pre = gate_pre.astype(BF16).astype(F32)
    up_pre = up_pre.astype(BF16).astype(F32)
    sigmoid = jax.nn.sigmoid(gate_pre)
    activated = gate_pre * sigmoid
    hidden = activated * up_pre
    gate_grad = (hidden_grad * up_pre * sigmoid * (1.0 + gate_pre * (1.0 - sigmoid))).astype(BF16)
    up_grad = (hidden_grad * activated).astype(BF16)
    return hidden, gate_grad, up_grad


def input_kernel(local_experts, quarter, landed, *refs):
    gates, ups, downs = refs[0:4], refs[4:8], refs[8:11]
    down_even, down_odd, out, rows, scaled, coded = refs[11:]
    own, _ = rows.shape
    slots = local_experts * quarter
    devices = own // quarter
    stride = (slots + 1) * SUBLANES
    expert = pl.program_id(0)

    @pl.when(expert == 0)
    def _():
        for i in range(slots, SUBLANES):
            at = slots * SUBLANES + i
            coded[pl.ds(at, devices, stride=stride), :] = jnp.zeros((devices, LANES), F32)

    land(landed, expert, local_experts, quarter, rows, scaled, 0)
    gate = jnp.concatenate([g[0] for g in gates], axis=1)
    up = jnp.concatenate([u[0] for u in ups], axis=1)
    last = jnp.where(expert == 0, down_even[0], down_odd[0])
    down = jnp.concatenate([d[0] for d in downs] + [last], axis=0)
    hidden_grad = mm(scaled[...], down, NT)
    hidden, gate_grad, up_grad = hidden_terms(mm(rows[...], gate), mm(rows[...], up), hidden_grad)
    product = jnp.sum(hidden_grad * hidden, axis=1, keepdims=True)
    grad = mm(gate_grad, gate, NT) + mm(up_grad, up, NT)
    grad, power, steps = code_rows(grad)
    lane = iota((own, LANES), 1)
    tail = jnp.zeros((own, LANES), F32)
    for at, column in enumerate((power, steps) + code_values(product)):
        tail = jnp.where(lane == at, column, tail)
    for block in range(devices // BLOCK):
        for q in range(quarter):
            at = (block * quarter + q) * BLOCK
            to = block * BLOCK * stride
            slot = expert * quarter + q
            for i in range(SUBLANES):
                piece = grad[at : at + BLOCK, i * LANES : (i + 1) * LANES]
                coded[pl.ds(to + slot * SUBLANES + i, BLOCK, stride=stride), :] = piece
            to += slots * SUBLANES + slot
            coded[pl.ds(to, BLOCK, stride=stride), :] = tail[at : at + BLOCK]

    @pl.when(expert == local_experts - 1)
    def _():
        out[...] = to_code(coded[...])


def weight_kernel(local_experts, quarter, source_count, earlier_count, *refs):
    sources, refs = refs[:source_count], refs[source_count:]
    (gate, up, down), refs = refs[:3], refs[3:]
    earlier, refs = refs[:earlier_count], refs[earlier_count:]
    outs, (rows, scaled) = refs[:3], refs[3:]
    chunk = HALVES * 2 * local_experts * quarter
    hidden_width = gate.shape[2]

    expert = pl.program_id(0)
    offset = 0
    for source in sources:
        land(source, expert, local_experts, quarter, rows, scaled, offset)
        offset += source.shape[0] // chunk * quarter
    both = mm(rows[...], jnp.concatenate([gate[0], up[0]], axis=1))
    hidden_grad = mm(scaled[...], down[0], NT)
    hidden, gate_grad, up_grad = hidden_terms(
        both[:, :hidden_width], both[:, hidden_width:], hidden_grad
    )
    grads = mm(rows[...], jnp.concatenate([gate_grad, up_grad], axis=1), TN)
    down_grad = mm(hidden.astype(BF16), scaled[...], TN)
    for at, part in enumerate((grads[:, :hidden_width], grads[:, hidden_width:], down_grad)):
        outs[at][0] = earlier[at][0] + part if earlier else part


def member_rows(member, distance, members, count):
    return pl.ds(pl.multiple_of(lax.rem(member + distance, members) * count, count), count)


def combine_kernel(members, devices, member, coded, pick, *refs):
    outs, total, back = refs[:-2], refs[-2], refs[-1]
    back[...] = from_code(coded[...])
    token_count, tail_width = total.shape
    width = tail_width - LANES
    slots = pick.shape[1] // devices
    stride = (slots + 1) * SUBLANES
    tails = [
        back[pl.ds(slots * SUBLANES + slot, devices, stride=stride), :] for slot in range(slots)
    ]
    tail = jnp.concatenate(tails, axis=0)
    scale = row_scale(tail[:, 0:1], tail[:, 1:2])
    columns = []
    for i in range(SUBLANES):
        pieces = [
            back[pl.ds(slot * SUBLANES + i, devices, stride=stride), :] for slot in range(slots)
        ]
        columns.append(jnp.concatenate(pieces, axis=0))
    grad = jnp.concatenate(columns, axis=1) * scale
    both = pick[0] + pick[1]
    grad, power, steps = code_rows(sum(mm(both, part, TN) for part in split3(grad)[:2]))
    total[:, 0:width] = grad
    lane = iota((token_count, LANES), 1)
    total[:, width:] = jnp.where(lane == 0, power, jnp.where(lane == 1, steps, 0.0))
    product = decode_values(tail[:, 2:3], tail[:, 3:4], tail[:, 4:5])
    sums = [jnp.sum(pick[k].astype(F32) * product, axis=0, keepdims=True) for k in range(2)]
    power, coarse, fine = code_values(jnp.concatenate(sums, axis=1))
    spare = jnp.zeros((1, tail_width - 4 * token_count), F32)
    first = jnp.concatenate([power, coarse, spare], axis=1)
    second = jnp.concatenate([fine, jnp.zeros_like(fine), spare], axis=1)
    line = iota((SUBLANES, tail_width), 0)
    lines = to_code(jnp.where(line == 0, first, jnp.where(line == 1, second, 0.0)))
    count = token_count // members
    for out, distance in zip(outs, (0, 1, 3, 2)):
        out[0:count, :] = to_code(total[member_rows(member[0], distance, members, count), :])
        out[count : count + SUBLANES, :] = lines


def sum_kernel(own, from_left, from_right, from_opposite, weights, grad_out, gates_out):
    count, width = grad_out.shape
    token_count = weights.shape[1]
    parts = [from_code(part[...]) for part in (own, from_left, from_right, from_opposite)]
    grads = [
        part[:count, :width] * row_scale(part[:count, width : width + 1], part[:count, width + 1 : width + 2])
        for part in parts
    ]
    grad_out[...] = ((grads[0] + grads[3]) + (grads[1] + grads[2])).astype(BF16)
    values = 2 * token_count
    products = [
        decode_values(
            part[count : count + 1, 0:values],
            part[count : count + 1, values : 2 * values],
            part[count + 1 : count + 2, 0:values],
        )
        for part in parts
    ]
    product = (products[0] + products[3]) + (products[1] + products[2])
    for k in range(2):
        gates_out[k : k + 1, :] = product[:, k * token_count : (k + 1) * token_count] / weights[k : k + 1, :]


def step(tokens, cotangent, routing, gate_weights, gate_proj, up_proj, down_proj):
    token_count, model_width = tokens.shape
    top_count = routing.shape[1]
    local_experts, _, hidden_width = gate_proj.shape
    groups = lax.axis_size("ep")
    members = lax.axis_size("tp")
    experts = local_experts * groups
    capacity = members * (
        (3 * token_count * top_count + experts * members - 1) // (experts * members)
    )
    quarter = capacity // members
    slots = experts * quarter
    own = groups * quarter
    chunk = HALVES * 2 * local_experts * quarter
    half = model_width // HALVES
    member = lax.axis_index("tp").astype(I32).reshape(1)
    right = [(i, (i + 1) % members) for i in range(members)]
    left = [(i, (i - 1) % members) for i in range(members)]
    across = [(i, (i + 2) % members) for i in range(members)]
    whole = pl.BlockSpec(memory_space=VMEM)
    scalar = pl.BlockSpec(memory_space=SMEM)

    def per_expert(array):
        return pl.BlockSpec((1,) + array.shape[1:], lambda e: (e, 0, 0))

    def constant(array):
        return pl.BlockSpec(array.shape, lambda e: (0,) * len(array.shape))

    def call(kernel, out_shape, args, scalars=0, scratch=(), specs=None):
        in_specs = [scalar] * scalars + [whole] * (len(args) - scalars)
        return pl.pallas_call(
            kernel,
            grid=(local_experts,) if specs else (),
            out_shape=out_shape,
            in_specs=specs[0] if specs else in_specs,
            out_specs=specs[1] if specs else jax.tree.map(lambda _: whole, out_shape),
            scratch_shapes=list(scratch),
        )(*args)

    def shape(dims, dtype):
        return jax.ShapeDtypeStruct(dims, dtype)

    gates, ups, downs = [gate_proj], [up_proj], [down_proj]
    for kept, mine in ((gates, gate_proj), (ups, up_proj), (downs, down_proj)):
        kept.append(lax.ppermute(mine, "tp", right))
        kept.append(lax.ppermute(mine, "tp", left))
    gates.append(lax.ppermute(gates[2], "tp", left))
    ups.append(lax.ppermute(ups[1], "tp", right))
    down_even = lax.ppermute(downs[2][0:1], "tp", left)
    down_odd = lax.ppermute(downs[1][1:2], "tp", right)

    send, pick = call(
        lambda *refs: dispatch_kernel(experts, local_experts, quarter, *refs),
        (shape((groups * chunk, half), BF16), shape((2, slots, token_count), BF16)),
        (member, routing.T, gate_weights.T, tokens, cotangent),
        scalars=1,
        scratch=[VMEM((half // LANES, groups * chunk, LANES), F32)],
    )
    landed = lax.all_to_all(
        send.reshape(groups, chunk, half), "ep", split_axis=0, concat_axis=0, tiled=True
    ).reshape(groups * chunk, half)

    middle = groups * chunk // 2
    low, high = landed[:middle], landed[middle:]
    left_high = lax.ppermute(high, "tp", right)
    right_low = lax.ppermute(low, "tp", left)
    right_high = lax.ppermute(high, "tp", left)
    left_low = lax.ppermute(low, "tp", right)
    opposite_low = lax.ppermute(right_low, "tp", left)
    opposite_high = lax.ppermute(left_high, "tp", right)

    back_rows = (local_experts * quarter + 1) * SUBLANES
    back = call(
        lambda *refs: input_kernel(local_experts, quarter, *refs),
        shape((groups * back_rows, LANES), I16),
        (landed, *gates, *ups, *downs, down_even, down_odd),
        scratch=[VMEM((own, model_width), BF16)] * 2 + [VMEM((groups * back_rows, LANES), F32)],
        specs=(
            [constant(landed)]
            + [per_expert(a) for a in (*gates, *ups, *downs)]
            + [constant(down_even), constant(down_odd)],
            pl.BlockSpec((groups * back_rows, LANES), lambda e: (0, 0)),
        ),
    )
    back = back.reshape(groups, back_rows, LANES)
    back = lax.all_to_all(back, "ep", split_axis=0, concat_axis=0, tiled=True)
    back = back.reshape(groups * back_rows, LANES)
    count = token_count // members
    tail_width = model_width + LANES
    part = shape((count + SUBLANES, tail_width), I16)
    mine, to_right, to_left, to_across = call(
        lambda *refs: combine_kernel(members, groups, *refs),
        (part,) * 4,
        (member, back, pick),
        scalars=1,
        scratch=[VMEM((token_count, tail_width), F32), VMEM((groups * back_rows, LANES), F32)],
    )
    pieces = (
        lax.ppermute(to_right, "tp", right),
        lax.ppermute(to_left, "tp", left),
        lax.ppermute(to_across, "tp", across),
    )
    summed, gates_grad = call(
        sum_kernel,
        (shape((count, model_width), BF16), shape((top_count, token_count), F32)),
        (mine, *pieces, gate_weights.T),
    )
    pieces = (
        lax.ppermute(summed, "tp", right),
        lax.ppermute(summed, "tp", left),
        lax.ppermute(summed, "tp", across),
    )
    tokens_grad = jnp.zeros((token_count, model_width), BF16)
    from_left_sum, from_right_sum, from_across_sum = pieces
    placed = ((summed, 0), (from_left_sum, 3), (from_right_sum, 1), (from_across_sum, 2))
    for piece, distance in placed:
        at = lax.rem(member[0] + distance, members) * count
        tokens_grad = lax.dynamic_update_slice(tokens_grad, piece, (at, 0))

    sums = (
        shape((local_experts, model_width, hidden_width), F32),
        shape((local_experts, model_width, hidden_width), F32),
        shape((local_experts, hidden_width, model_width), F32),
    )

    def weight_sums(sources, earlier):
        count = sum(source.shape[0] for source in sources) // chunk * quarter
        shared = (gate_proj, up_proj, down_proj, *earlier)
        return call(
            lambda *refs: weight_kernel(local_experts, quarter, len(sources), len(earlier), *refs),
            sums,
            (*sources, *shared),
            scratch=[VMEM((count, model_width), BF16)] * 2,
            specs=(
                [constant(a) for a in sources] + [per_expert(a) for a in shared],
                tuple(per_expert(a) for a in sums),
            ),
        )

    near = weight_sums((landed, right_low, left_high), ())
    mid = weight_sums((right_high, left_low), near)
    gate_grad, up_grad, down_grad = weight_sums((opposite_low, opposite_high), mid)
    return (tokens_grad, gates_grad.T, gate_grad, up_grad, down_grad)


def solution(mesh):
    in_specs = (
        P("ep", None),
        P("ep", None),
        P("ep", None),
        P("ep", None),
        P("ep", None, "tp"),
        P("ep", None, "tp"),
        P("ep", "tp", None),
    )
    out_specs = (
        P("ep", None),
        P("ep", None),
        P("ep", None, "tp"),
        P("ep", None, "tp"),
        P("ep", "tp", None),
    )
    return jax.shard_map(step, mesh=mesh, in_specs=in_specs, out_specs=out_specs, check_vma=False)
```

profile of v0, /device:TPU:14, one launch (start us, length us, event | category | flops | bytes accessed | tf_op | source)
XLA Modules:
  0.0 200.0 jit_solution(14057476279392598483)
XLA Ops:
  0.6 3.8 %shard_map.110 = (bf16[1536,512]{1,0:T(8,128)(2,1)}, bf16[2,384,256]{2,1,0:T(8,128)(2,1)}) custom-call(s32[1]{0:T(128)} %bitcast.refs_0_, s32[2,256]{1,0:T(2,128)} %bitcast.17, f32[2,256]{1,0:T(2,128)} %bitcast.15, bf16[256,1024]{1,0:T(8,128)(2,1)} %refs_3_.4, bf16[256,1024]{1,0:T(8,128)(2,1)} %refs_4_.4), custom_call_target="tpu_custom_call" | custom-call | tf_op jit(solution)/shard_map/pallas_call | solution.py:317
  4.4 12.2 %all-to-all-start = ((bf16[64,24,512]{2,1,0:T(8,128)(2,1)}), bf16[64,24,512]{2,1,0:T(8,128)(2,1)S(1)}, u32[]{:S(2)}, u32[]{:S(2)}) async-start(bf16[64,24,512]{2,1,0:T(8,128)(2,1)} %bitcast.14), calls=%async_computation | async-start | bytes 3145728 | tf_op jit(solution)/shard_map/all_to_all | solution.py:345
  17.6 2.4 %collective-permute-start.3 = (bf16[2,1024,128]{2,1,0:T(8,128)(2,1)S(1)}, bf16[2,1024,128]{2,1,0:T(8,128)(2,1)S(1)}, u32[]{:S(2)}, u32[]{:S(2)}) collective-permute-start(bf16[2,1024,128]{2,1,0:T(8,128)(2,1)S(1)} %copy-done.3), channel_id=1, source_target_pairs={{0,1},{1,2},{2,3},{3,0},{4,5},{5,6},{6,7},{7,4},{8,9},{9,10},{10,1... | collective-permute-start | bytes 1572872 | tf_op jit(solution)/shard_map/ppermute | solution.py:331
  20.0 3.2 %collective-permute-start.6 = (bf16[2,128,1024]{2,1,0:T(8,128)(2,1)S(1)}, bf16[2,128,1024]{2,1,0:T(8,128)(2,1)S(1)}, u32[]{:S(2)}, u32[]{:S(2)}) collective-permute-start(bf16[2,128,1024]{2,1,0:T(8,128)(2,1)S(1)} %copy-done.4), channel_id=1, source_target_pairs={{0,1},{1,2},{2,3},{3,0},{4,5},{5,6},{6,7},{7,4},{8,9},{9,10},{10,1... | collective-permute-start | bytes 1572872 | tf_op jit(solution)/shard_map/ppermute | solution.py:331
  23.2 9.5 %collective-permute-done.1.refs_3_ = bf16[2,1024,128]{2,1,0:T(8,128)(2,1)S(1)} collective-permute-done((bf16[2,1024,128]{2,1,0:T(8,128)(2,1)S(1)}, bf16[2,1024,128]{2,1,0:T(8,128)(2,1)S(1)}, u32[]{:S(2)}, u32[]{:S(2)}) %collective-permute-start.1) | collective-permute-done | bytes 524320 | tf_op jit(solution)/shard_map/ppermute | solution.py:332
  32.9 11.1 %collective-permute-done.7.refs_11_ = bf16[2,128,1024]{2,1,0:T(8,128)(2,1)S(1)} collective-permute-done((bf16[2,128,1024]{2,1,0:T(8,128)(2,1)S(1)}, bf16[2,128,1024]{2,1,0:T(8,128)(2,1)S(1)}, u32[]{:S(2)}, u32[]{:S(2)}) %collective-permute-start.7) | collective-permute-done | bytes 524320 | tf_op jit(solution)/shard_map/ppermute | solution.py:332
  44.0 2.1 %collective-permute-start.8 = (bf16[1,128,1024]{2,1,0:T(8,128)(2,1)S(1)}, bf16[1,128,1024]{2,1,0:T(8,128)(2,1)S(1)}, u32[]{:S(2)}, u32[]{:S(2)}) collective-permute-start(bf16[1,128,1024]{2,1,0:T(8,128)(2,1)S(1)} %slice.24), channel_id=1, source_target_pairs={{0,3},{1,0},{2,1},{3,2},{4,7},{5,4},{6,5},{7,6},{8,11},{9,8},{10,9... | collective-permute-start | bytes 786440 | tf_op jit(solution)/shard_map/ppermute | solution.py:335
  46.1 8.7 %collective-permute-done.refs_2_ = bf16[2,1024,128]{2,1,0:T(8,128)(2,1)S(1)} collective-permute-done((bf16[2,1024,128]{2,1,0:T(8,128)(2,1)S(1)}, bf16[2,1024,128]{2,1,0:T(8,128)(2,1)S(1)}, u32[]{:S(2)}, u32[]{:S(2)}) %collective-permute-start) | collective-permute-done | bytes 524320 | tf_op jit(solution)/shard_map/ppermute | solution.py:331
  54.8 3.6 %collective-permute-start.9 = (bf16[1,128,1024]{2,1,0:T(8,128)(2,1)S(1)}, bf16[1,128,1024]{2,1,0:T(8,128)(2,1)S(1)}, u32[]{:S(2)}, u32[]{:S(2)}) collective-permute-start(bf16[1,128,1024]{2,1,0:T(8,128)(2,1)S(1)} %slice.25), channel_id=1, source_target_pairs={{0,1},{1,2},{2,3},{3,0},{4,5},{5,6},{6,7},{7,4},{8,9},{9,10},{10,1... | collective-permute-start | bytes 786440 | tf_op jit(solution)/shard_map/ppermute | solution.py:336
  58.5 12.8 %collective-permute-done.8.refs_12_ = bf16[1,128,1024]{2,1,0:T(8,128)(2,1)S(1)} collective-permute-done((bf16[1,128,1024]{2,1,0:T(8,128)(2,1)S(1)}, bf16[1,128,1024]{2,1,0:T(8,128)(2,1)S(1)}, u32[]{:S(2)}, u32[]{:S(2)}) %collective-permute-start.8) | collective-permute-done | bytes 262176 | tf_op jit(solution)/shard_map/ppermute | solution.py:335
  73.3 8.9 %shard_map.111 = s16[3584,128]{1,0:T(8,128)(2,1)} custom-call(bf16[1536,512]{1,0:T(8,128)(2,1)} %bitcast.10, bf16[2,1024,128]{2,1,0:T(8,128)(2,1)} %refs_2_.3, bf16[2,1024,128]{2,1,0:T(8,128)(2,1)} %copy-done.13, bf16[2,1024,128]{2,1,0:T(8,128)(2,1)} %copy-done.11, bf16[2,1024,128]{2,1,0:T(8,128)(2,1)} %copy-done.15, bf16[2,1024,128]{2,1,0:T(8,128)(2,1)} %refs_3_.7, ...), custom_call_target="tpu_custom_call" | custom-call | tf_op jit(solution)/shard_map/pallas_call | solution.py:317
  82.2 10.6 %all-to-all-start.1 = ((s16[64,56,128]{2,1,0:T(8,128)(2,1)}), s16[64,56,128]{2,1,0:T(8,128)(2,1)S(1)}, u32[]{:S(2)}, u32[]{:S(2)}) async-start(s16[64,56,128]{2,1,0:T(8,128)(2,1)} %bitcast.12), calls=%async_computation.1 | async-start | bytes 1835008 | tf_op jit(solution)/shard_map/all_to_all | solution.py:372
  94.1 3.2 %collective-permute-start.18 = (bf16[768,512]{1,0:T(8,128)(2,1)}, bf16[768,512]{1,0:T(8,128)(2,1)S(1)}, u32[]{:S(2)}, u32[]{:S(2)}) collective-permute-start(bf16[768,512]{1,0:T(8,128)(2,1)} %bitcast.9), channel_id=1, source_target_pairs={{0,1},{1,2},{2,3},{3,0},{4,5},{5,6},{6,7},{7,4},{8,9},{9,10},{10,1... | collective-permute-start | bytes 2359304 | tf_op jit(solution)/shard_map/ppermute | solution.py:351
  99.3 16.6 %collective-permute-done.16.refs_1_ = bf16[768,512]{1,0:T(8,128)(2,1)S(1)} collective-permute-done((bf16[768,512]{1,0:T(8,128)(2,1)}, bf16[768,512]{1,0:T(8,128)(2,1)S(1)}, u32[]{:S(2)}, u32[]{:S(2)}) %collective-permute-start.16) | collective-permute-done | bytes 786464 | tf_op jit(solution)/shard_map/ppermute | solution.py:352
  115.9 3.2 %collective-permute-start.19 = (bf16[768,512]{1,0:T(8,128)(2,1)S(1)}, bf16[768,512]{1,0:T(8,128)(2,1)}, u32[]{:S(2)}, u32[]{:S(2)}) collective-permute-start(bf16[768,512]{1,0:T(8,128)(2,1)S(1)} %collective-permute-done.18.refs_2_), channel_id=1, source_target_pairs={{0,1},{1,2},{2,3},{3,0},{4,5},{5,6},{6,7},{7,4},{8,9},{9,10},{10,1... | collective-permute-start | bytes 2359304 | tf_op jit(solution)/shard_map/ppermute | solution.py:356
  120.1 3.6 %shard_map.112 = (s16[72,1152]{1,0:T(8,128)(2,1)}, s16[72,1152]{1,0:T(8,128)(2,1)}, s16[72,1152]{1,0:T(8,128)(2,1)}, s16[72,1152]{1,0:T(8,128)(2,1)}) custom-call(s32[1]{0:T(128)} %bitcast.refs_0_, s16[3584,128]{1,0:T(8,128)(2,1)} %bitcast.13, bf16[2,384,256]{2,1,0:T(8,128)(2,1)} %get-tuple-element.23.refs_2_), custom_call_target="tpu_custom_call" | custom-call | tf_op jit(solution)/shard_map/pallas_call | solution.py:317
  123.7 2.5 %collective-permute-start.10 = (s16[72,1152]{1,0:T(8,128)(2,1)}, s16[72,1152]{1,0:T(8,128)(2,1)S(1)}, u32[]{:S(2)}, u32[]{:S(2)}) collective-permute-start(s16[72,1152]{1,0:T(8,128)(2,1)} %get-tuple-element.25), channel_id=1, source_target_pairs={{0,1},{1,2},{2,3},{3,0},{4,5},{5,6},{6,7},{7,4},{8,9},{9,10},{10,1... | collective-permute-start | bytes 497672 | tf_op jit(solution)/shard_map/ppermute | solution.py:385
  126.3 25.4 %collective-permute-done.10.from_left = s16[72,1152]{1,0:T(8,128)(2,1)S(1)} collective-permute-done((s16[72,1152]{1,0:T(8,128)(2,1)}, s16[72,1152]{1,0:T(8,128)(2,1)S(1)}, u32[]{:S(2)}, u32[]{:S(2)}) %collective-permute-start.10) | collective-permute-done | bytes 165920 | tf_op jit(solution)/shard_map/ppermute | solution.py:385
  153.4 5.5 %collective-permute-done.11.from_right = s16[72,1152]{1,0:T(8,128)(2,1)S(1)} collective-permute-done((s16[72,1152]{1,0:T(8,128)(2,1)}, s16[72,1152]{1,0:T(8,128)(2,1)S(1)}, u32[]{:S(2)}, u32[]{:S(2)}) %collective-permute-start.11) | collective-permute-done | bytes 165920 | tf_op jit(solution)/shard_map/ppermute | solution.py:386
  160.8 5.2 %collective-permute-done.12.from_opposite = s16[72,1152]{1,0:T(8,128)(2,1)S(1)} collective-permute-done((s16[72,1152]{1,0:T(8,128)(2,1)}, s16[72,1152]{1,0:T(8,128)(2,1)S(1)}, u32[]{:S(2)}, u32[]{:S(2)}) %collective-permute-start.12) | collective-permute-done | bytes 165920 | tf_op jit(solution)/shard_map/ppermute | solution.py:387
  170.6 7.3 %shard_map.114 = (f32[2,1024,128]{2,1,0:T(8,128)}, f32[2,1024,128]{2,1,0:T(8,128)}, f32[2,128,1024]{2,1,0:T(8,128)}) custom-call(bf16[1536,512]{1,0:T(8,128)(2,1)} %bitcast.11, bf16[768,512]{1,0:T(8,128)(2,1)} %copy-done.8, bf16[768,512]{1,0:T(8,128)(2,1)} %copy-done.9, bf16[2,1024,128]{2,1,0:T(8,128)(2,1)} %refs_2_.3, bf16[2,1024,128]{2,1,0:T(8,128)(2,1)} %refs_3_.7, ...), custom_call_target="tpu_custom_call" | custom-call | tf_op jit(solution)/shard_map/pallas_call | solution.py:317
  177.9 6.2 %shard_map.115 = (f32[2,1024,128]{2,1,0:T(8,128)}, f32[2,1024,128]{2,1,0:T(8,128)}, f32[2,128,1024]{2,1,0:T(8,128)}) custom-call(bf16[768,512]{1,0:T(8,128)(2,1)} %collective-permute-done.20.refs_0_, bf16[768,512]{1,0:T(8,128)(2,1)} %collective-permute-done.21.refs_1_, bf16[2,1024,128]{2,1,0:T(8,128)(2,1)} %refs_2_.3, bf16[2,1024,128]{2,1,0:T(8,128)(2,1)} %refs_3_.7, ...), custom_call_target="tpu_custom_call" | custom-call | tf_op jit(solution)/shard_map/pallas_call | solution.py:317
  185.0 6.2 %shard_map.116 = (f32[2,1024,128]{2,1,0:T(8,128)}, f32[2,1024,128]{2,1,0:T(8,128)}, f32[2,128,1024]{2,1,0:T(8,128)}) custom-call(bf16[768,512]{1,0:T(8,128)(2,1)} %copy-done.10, bf16[768,512]{1,0:T(8,128)(2,1)} %collective-permute-done.19.refs_1_, bf16[2,1024,128]{2,1,0:T(8,128)(2,1)} %refs_2_.3, bf16[2,1024,128]{2,1,0:T(8,128)(2,1)} %refs_3_.7, ...), custom_call_target="tpu_custom_call" | custom-call | tf_op jit(solution)/shard_map/pallas_call | solution.py:317
  192.8 6.4 %collective-permute-done.14 = bf16[64,1024]{1,0:T(8,128)(2,1)S(1)} collective-permute-done((bf16[64,1024]{1,0:T(8,128)(2,1)S(1)}, bf16[64,1024]{1,0:T(8,128)(2,1)S(1)}, u32[]{:S(2)}, u32[]{:S(2)}) %collective-permute-start.14) | collective-permute-done | bytes 131104 | tf_op jit(solution)/shard_map/ppermute | solution.py:396
  (85 shorter events, 18.9 us)
Async XLA Ops:
  4.4 67.8 %all-to-all-start = ((bf16[64,24,512]{2,1,0:T(8,128)(2,1)}), bf16[64,24,512]{2,1,0:T(8,128)(2,1)S(1)}, u32[]{:S(2)}, u32[]{:S(2)}) async-start(bf16[64,24,512]{2,1,0:T(8,128)(2,1)} %bitcast.14), calls=%async_computation | async-start | bytes 3145728 | tf_op jit(solution)/shard_map/all_to_all | solution.py:345
  16.7 16.1 %collective-permute-start.1 = (bf16[2,1024,128]{2,1,0:T(8,128)(2,1)S(1)}, bf16[2,1024,128]{2,1,0:T(8,128)(2,1)S(1)}, u32[]{:S(2)}, u32[]{:S(2)}) collective-permute-start(bf16[2,1024,128]{2,1,0:T(8,128)(2,1)S(1)} %copy-done.2), channel_id=1, source_target_pairs={{0,3},{1,0},{2,1},{3,2},{4,7},{5,4},{6,5},{7,6},{8,11},{9,8},{10,9... | collective-permute-start | bytes 1572872 | tf_op jit(solution)/shard_map/ppermute | solution.py:332
  17.6 15.2 %collective-permute-start.3 = (bf16[2,1024,128]{2,1,0:T(8,128)(2,1)S(1)}, bf16[2,1024,128]{2,1,0:T(8,128)(2,1)S(1)}, u32[]{:S(2)}, u32[]{:S(2)}) collective-permute-start(bf16[2,1024,128]{2,1,0:T(8,128)(2,1)S(1)} %copy-done.3), channel_id=1, source_target_pairs={{0,1},{1,2},{2,3},{3,0},{4,5},{5,6},{6,7},{7,4},{8,9},{9,10},{10,1... | collective-permute-start | bytes 1572872 | tf_op jit(solution)/shard_map/ppermute | solution.py:331
  20.0 24.0 %collective-permute-start.7 = (bf16[2,128,1024]{2,1,0:T(8,128)(2,1)S(1)}, bf16[2,128,1024]{2,1,0:T(8,128)(2,1)S(1)}, u32[]{:S(2)}, u32[]{:S(2)}) collective-permute-start(bf16[2,128,1024]{2,1,0:T(8,128)(2,1)S(1)} %copy-done.4), channel_id=1, source_target_pairs={{0,3},{1,0},{2,1},{3,2},{4,7},{5,4},{6,5},{7,6},{8,11},{9,8},{10,9... | collective-permute-start | bytes 1572872 | tf_op jit(solution)/shard_map/ppermute | solution.py:332
  20.0 24.0 %collective-permute-start.6 = (bf16[2,128,1024]{2,1,0:T(8,128)(2,1)S(1)}, bf16[2,128,1024]{2,1,0:T(8,128)(2,1)S(1)}, u32[]{:S(2)}, u32[]{:S(2)}) collective-permute-start(bf16[2,128,1024]{2,1,0:T(8,128)(2,1)S(1)} %copy-done.4), channel_id=1, source_target_pairs={{0,1},{1,2},{2,3},{3,0},{4,5},{5,6},{6,7},{7,4},{8,9},{9,10},{10,1... | collective-permute-start | bytes 1572872 | tf_op jit(solution)/shard_map/ppermute | solution.py:331
  23.2 31.6 %collective-permute-start = (bf16[2,1024,128]{2,1,0:T(8,128)(2,1)S(1)}, bf16[2,1024,128]{2,1,0:T(8,128)(2,1)S(1)}, u32[]{:S(2)}, u32[]{:S(2)}) collective-permute-start(bf16[2,1024,128]{2,1,0:T(8,128)(2,1)S(1)} %copy-done.2), channel_id=1, source_target_pairs={{0,1},{1,2},{2,3},{3,0},{4,5},{5,6},{6,7},{7,4},{8,9},{9,10},{10,1... | collective-permute-start | bytes 1572872 | tf_op jit(solution)/shard_map/ppermute | solution.py:331
  32.7 25.7 %collective-permute-start.4 = (bf16[2,1024,128]{2,1,0:T(8,128)(2,1)S(1)}, bf16[2,1024,128]{2,1,0:T(8,128)(2,1)S(1)}, u32[]{:S(2)}, u32[]{:S(2)}) collective-permute-start(bf16[2,1024,128]{2,1,0:T(8,128)(2,1)S(1)} %copy-done.3), channel_id=1, source_target_pairs={{0,3},{1,0},{2,1},{3,2},{4,7},{5,4},{6,5},{7,6},{8,11},{9,8},{10,9... | collective-permute-start | bytes 1572872 | tf_op jit(solution)/shard_map/ppermute | solution.py:332
  32.8 38.5 %collective-permute-start.2 = (bf16[2,1024,128]{2,1,0:T(8,128)(2,1)S(1)}, bf16[2,1024,128]{2,1,0:T(8,128)(2,1)S(1)}, u32[]{:S(2)}, u32[]{:S(2)}) collective-permute-start(bf16[2,1024,128]{2,1,0:T(8,128)(2,1)S(1)} %collective-permute-done.1.refs_3_), channel_id=1, source_target_pairs={{0,3},{1,0},{2,1},{3,2},{4,7},{5,4},{6,5},{7,6},{8,11},{9,8},{10,9... | collective-permute-start | bytes 1572872 | tf_op jit(solution)/shard_map/ppermute | solution.py:333
  44.0 28.2 %collective-permute-start.5 = (bf16[2,1024,128]{2,1,0:T(8,128)(2,1)S(1)}, bf16[2,1024,128]{2,1,0:T(8,128)(2,1)}, u32[]{:S(2)}, u32[]{:S(2)}) collective-permute-start(bf16[2,1024,128]{2,1,0:T(8,128)(2,1)S(1)} %collective-permute-done.3.refs_6_), channel_id=1, source_target_pairs={{0,1},{1,2},{2,3},{3,0},{4,5},{5,6},{6,7},{7,4},{8,9},{9,10},{10,1... | collective-permute-start | bytes 1572872 | tf_op jit(solution)/shard_map/ppermute | solution.py:334
  44.0 27.2 %collective-permute-start.8 = (bf16[1,128,1024]{2,1,0:T(8,128)(2,1)S(1)}, bf16[1,128,1024]{2,1,0:T(8,128)(2,1)S(1)}, u32[]{:S(2)}, u32[]{:S(2)}) collective-permute-start(bf16[1,128,1024]{2,1,0:T(8,128)(2,1)S(1)} %slice.24), channel_id=1, source_target_pairs={{0,3},{1,0},{2,1},{3,2},{4,7},{5,4},{6,5},{7,6},{8,11},{9,8},{10,9... | collective-permute-start | bytes 786440 | tf_op jit(solution)/shard_map/ppermute | solution.py:335
  54.8 16.4 %collective-permute-start.9 = (bf16[1,128,1024]{2,1,0:T(8,128)(2,1)S(1)}, bf16[1,128,1024]{2,1,0:T(8,128)(2,1)S(1)}, u32[]{:S(2)}, u32[]{:S(2)}) collective-permute-start(bf16[1,128,1024]{2,1,0:T(8,128)(2,1)S(1)} %slice.25), channel_id=1, source_target_pairs={{0,1},{1,2},{2,3},{3,0},{4,5},{5,6},{6,7},{7,4},{8,9},{9,10},{10,1... | collective-permute-start | bytes 786440 | tf_op jit(solution)/shard_map/ppermute | solution.py:336
  82.2 37.0 %all-to-all-start.1 = ((s16[64,56,128]{2,1,0:T(8,128)(2,1)}), s16[64,56,128]{2,1,0:T(8,128)(2,1)S(1)}, u32[]{:S(2)}, u32[]{:S(2)}) async-start(s16[64,56,128]{2,1,0:T(8,128)(2,1)} %bitcast.12), calls=%async_computation.1 | async-start | bytes 1835008 | tf_op jit(solution)/shard_map/all_to_all | solution.py:372
  94.1 21.8 %collective-permute-start.16 = (bf16[768,512]{1,0:T(8,128)(2,1)}, bf16[768,512]{1,0:T(8,128)(2,1)S(1)}, u32[]{:S(2)}, u32[]{:S(2)}) collective-permute-start(bf16[768,512]{1,0:T(8,128)(2,1)} %bitcast.8), channel_id=1, source_target_pairs={{0,3},{1,0},{2,1},{3,2},{4,7},{5,4},{6,5},{7,6},{8,11},{9,8},{10,9... | collective-permute-start | bytes 2359304 | tf_op jit(solution)/shard_map/ppermute | solution.py:352
  94.1 21.8 %collective-permute-start.18 = (bf16[768,512]{1,0:T(8,128)(2,1)}, bf16[768,512]{1,0:T(8,128)(2,1)S(1)}, u32[]{:S(2)}, u32[]{:S(2)}) collective-permute-start(bf16[768,512]{1,0:T(8,128)(2,1)} %bitcast.9), channel_id=1, source_target_pairs={{0,1},{1,2},{2,3},{3,0},{4,5},{5,6},{6,7},{7,4},{8,9},{9,10},{10,1... | collective-permute-start | bytes 2359304 | tf_op jit(solution)/shard_map/ppermute | solution.py:351
  97.3 80.6 %collective-permute-start.21 = (bf16[768,512]{1,0:T(8,128)(2,1)}, bf16[768,512]{1,0:T(8,128)(2,1)}, u32[]{:S(2)}, u32[]{:S(2)}) collective-permute-start(bf16[768,512]{1,0:T(8,128)(2,1)} %bitcast.8), channel_id=1, source_target_pairs={{0,1},{1,2},{2,3},{3,0},{4,5},{5,6},{6,7},{7,4},{8,9},{9,10},{10,1... | collective-permute-start | bytes 2359304 | tf_op jit(solution)/shard_map/ppermute | solution.py:354
  99.0 78.9 %collective-permute-start.20 = (bf16[768,512]{1,0:T(8,128)(2,1)}, bf16[768,512]{1,0:T(8,128)(2,1)}, u32[]{:S(2)}, u32[]{:S(2)}) collective-permute-start(bf16[768,512]{1,0:T(8,128)(2,1)} %bitcast.9), channel_id=1, source_target_pairs={{0,3},{1,0},{2,1},{3,2},{4,7},{5,4},{6,5},{7,6},{8,11},{9,8},{10,9... | collective-permute-start | bytes 2359304 | tf_op jit(solution)/shard_map/ppermute | solution.py:353
  115.9 68.2 %collective-permute-start.17 = (bf16[768,512]{1,0:T(8,128)(2,1)S(1)}, bf16[768,512]{1,0:T(8,128)(2,1)S(1)}, u32[]{:S(2)}, u32[]{:S(2)}) collective-permute-start(bf16[768,512]{1,0:T(8,128)(2,1)S(1)} %collective-permute-done.16.refs_1_), channel_id=1, source_target_pairs={{0,3},{1,0},{2,1},{3,2},{4,7},{5,4},{6,5},{7,6},{8,11},{9,8},{10,9... | collective-permute-start | bytes 2359304 | tf_op jit(solution)/shard_map/ppermute | solution.py:355
  115.9 68.2 %collective-permute-start.19 = (bf16[768,512]{1,0:T(8,128)(2,1)S(1)}, bf16[768,512]{1,0:T(8,128)(2,1)}, u32[]{:S(2)}, u32[]{:S(2)}) collective-permute-start(bf16[768,512]{1,0:T(8,128)(2,1)S(1)} %collective-permute-done.18.refs_2_), channel_id=1, source_target_pairs={{0,1},{1,2},{2,3},{3,0},{4,5},{5,6},{6,7},{7,4},{8,9},{9,10},{10,1... | collective-permute-start | bytes 2359304 | tf_op jit(solution)/shard_map/ppermute | solution.py:356
  123.7 28.0 %collective-permute-start.10 = (s16[72,1152]{1,0:T(8,128)(2,1)}, s16[72,1152]{1,0:T(8,128)(2,1)S(1)}, u32[]{:S(2)}, u32[]{:S(2)}) collective-permute-start(s16[72,1152]{1,0:T(8,128)(2,1)} %get-tuple-element.25), channel_id=1, source_target_pairs={{0,1},{1,2},{2,3},{3,0},{4,5},{5,6},{6,7},{7,4},{8,9},{9,10},{10,1... | collective-permute-start | bytes 497672 | tf_op jit(solution)/shard_map/ppermute | solution.py:385
  151.7 7.2 %collective-permute-start.11 = (s16[72,1152]{1,0:T(8,128)(2,1)}, s16[72,1152]{1,0:T(8,128)(2,1)S(1)}, u32[]{:S(2)}, u32[]{:S(2)}) collective-permute-start(s16[72,1152]{1,0:T(8,128)(2,1)} %get-tuple-element.26), channel_id=1, source_target_pairs={{0,3},{1,0},{2,1},{3,2},{4,7},{5,4},{6,5},{7,6},{8,11},{9,8},{10,9... | collective-permute-start | bytes 497672 | tf_op jit(solution)/shard_map/ppermute | solution.py:386
  158.9 7.1 %collective-permute-start.12 = (s16[72,1152]{1,0:T(8,128)(2,1)}, s16[72,1152]{1,0:T(8,128)(2,1)S(1)}, u32[]{:S(2)}, u32[]{:S(2)}) collective-permute-start(s16[72,1152]{1,0:T(8,128)(2,1)} %get-tuple-element.27), channel_id=1, source_target_pairs={{0,2},{1,3},{2,0},{3,1},{4,6},{5,7},{6,4},{7,5},{8,10},{9,11},{10,... | collective-permute-start | bytes 497672 | tf_op jit(solution)/shard_map/ppermute | solution.py:387
  168.6 24.1 %collective-permute-start.13 = (bf16[64,1024]{1,0:T(8,128)(2,1)}, bf16[64,1024]{1,0:T(8,128)(2,1)S(1)}, u32[]{:S(2)}, u32[]{:S(2)}) collective-permute-start(bf16[64,1024]{1,0:T(8,128)(2,1)} %get-tuple-element.28), channel_id=1, source_target_pairs={{0,1},{1,2},{2,3},{3,0},{4,5},{5,6},{6,7},{7,4},{8,9},{9,10},{10,1... | collective-permute-start | bytes 393224 | tf_op jit(solution)/shard_map/ppermute | solution.py:395
  191.3 8.0 %collective-permute-start.15 = (bf16[64,1024]{1,0:T(8,128)(2,1)S(1)}, bf16[64,1024]{1,0:T(8,128)(2,1)S(1)}, u32[]{:S(2)}, u32[]{:S(2)}) collective-permute-start(bf16[64,1024]{1,0:T(8,128)(2,1)S(1)} %copy-done.22), channel_id=1, source_target_pairs={{0,2},{1,3},{2,0},{3,1},{4,6},{5,7},{6,4},{7,5},{8,10},{9,11},{10,... | collective-permute-start | bytes 393224 | tf_op jit(solution)/shard_map/ppermute | solution.py:397
  191.6 7.6 %collective-permute-start.14 = (bf16[64,1024]{1,0:T(8,128)(2,1)S(1)}, bf16[64,1024]{1,0:T(8,128)(2,1)S(1)}, u32[]{:S(2)}, u32[]{:S(2)}) collective-permute-start(bf16[64,1024]{1,0:T(8,128)(2,1)S(1)} %copy-done.22), channel_id=1, source_target_pairs={{0,3},{1,0},{2,1},{3,2},{4,7},{5,4},{6,5},{7,6},{8,11},{9,8},{10,9... | collective-permute-start | bytes 393224 | tf_op jit(solution)/shard_map/ppermute | solution.py:396
  (23 other events, 356.6 us)
where the time goes:
time: 201 us; the launch traced here: 200 us
  waiting for transfers between devices  101 us (50%)
  starting transfers between devices  53.3 us (27%)
  Pallas kernels  38 us (19%)
  local copies, waits for them, and re-layouts  6.72 us (3%)
    pallas_call x7, Pallas kernels, call(): pl.pallas_call(kernel, grid=(local_experts,) if specs else (), out_shape=...  38 us
    ppermute x1, waiting for transfers between devices, step(): lax.ppermute(to_right, 'tp', right)  25.4 us
    ppermute x3, waiting for transfers between devices, step(): kept.append(lax.ppermute(mine, 'tp', left))  20.6 us
    ppermute x1, waiting for transfers between devices, step(): right_low = lax.ppermute(low, 'tp', left)  16.6 us
    ppermute x1, waiting for transfers between devices, step(): down_even = lax.ppermute(downs[2][0:1], 'tp', left)  12.8 us
    all_to_all x1, starting transfers between devices, step(): lax.all_to_all(send.reshape(groups, chunk, half), 'ep', split_axis=0, con...  12.2 us
    all_to_all x1, starting transfers between devices, step(): back = lax.all_to_all(back, 'ep', split_axis=0, concat_axis=0, tiled=True)  10.6 us
    ppermute x3, waiting for transfers between devices, step(): kept.append(lax.ppermute(mine, 'tp', right))  8.68 us
  transfers between devices with their start and end apart: 24, of which 9 were waited for; matrix products, arithmetic and copies ran while one was open for 1% of the time, Pallas kernels for 13%

commit v1 on v0

--- a/solution.py
+++ b/solution.py
@@ -381,20 +381,22 @@
         scalars=1,
         scratch=[VMEM((token_count, tail_width), F32), VMEM((groups * back_rows, LANES), F32)],
     )
+    far_piece = lax.ppermute(to_across, "tp", across)
     pieces = (
         lax.ppermute(to_right, "tp", right),
         lax.ppermute(to_left, "tp", left),
-        lax.ppermute(to_across, "tp", across),
+        far_piece,
     )
     summed, gates_grad = call(
         sum_kernel,
         (shape((count, model_width), BF16), shape((top_count, token_count), F32)),
         (mine, *pieces, gate_weights.T),
     )
+    far_piece = lax.ppermute(summed, "tp", across)
     pieces = (
         lax.ppermute(summed, "tp", right),
         lax.ppermute(summed, "tp", left),
-        lax.ppermute(summed, "tp", across),
+        far_piece,
     )
     tokens_grad = jnp.zeros((token_count, model_width), BF16)
     from_left_sum, from_right_sum, from_across_sum = pieces

time: 201 us -> 201 us (level)
  no operation moved by 1% of the time
where the time goes in v1:
time: 201 us; the launch traced here: 200 us
  waiting for transfers between devices  101 us (50%)
  starting transfers between devices  53.3 us (27%)
  Pallas kernels  38 us (19%)
  local copies, waits for them, and re-layouts  6.72 us (3%)
    pallas_call x7, Pallas kernels, call(): pl.pallas_call(kernel, grid=(local_experts,) if specs else (), out_shape=...  38 us
    ppermute x1, waiting for transfers between devices, step(): lax.ppermute(to_right, 'tp', right)  25.4 us
    ppermute x3, waiting for transfers between devices, step(): kept.append(lax.ppermute(mine, 'tp', left))  20.6 us
    ppermute x1, waiting for transfers between devices, step(): right_low = lax.ppermute(low, 'tp', left)  16.6 us
    ppermute x1, waiting for transfers between devices, step(): down_even = lax.ppermute(downs[2][0:1], 'tp', left)  12.8 us
    all_to_all x1, starting transfers between devices, step(): lax.all_to_all(send.reshape(groups, chunk, half), 'ep', split_axis=0, con...  12.2 us
    all_to_all x1, starting transfers between devices, step(): back = lax.all_to_all(back, 'ep', split_axis=0, concat_axis=0, tiled=True)  10.6 us
    ppermute x3, waiting for transfers between devices, step(): kept.append(lax.ppermute(mine, 'tp', right))  8.68 us
  transfers between devices with their start and end apart: 24, of which 9 were waited for; matrix products, arithmetic and copies ran while one was open for 1% of the time, Pallas kernels for 13%

profile of v1, /device:TPU:14, one launch (start us, length us, event | category | flops | bytes accessed | tf_op | source)
XLA Modules:
  0.0 200.0 jit_solution(14057476279392598483)
XLA Ops:
  0.6 3.8 %shard_map.110 = (bf16[1536,512]{1,0:T(8,128)(2,1)}, bf16[2,384,256]{2,1,0:T(8,128)(2,1)}) custom-call(s32[1]{0:T(128)} %bitcast.refs_0_, s32[2,256]{1,0:T(2,128)} %bitcast.17, f32[2,256]{1,0:T(2,128)} %bitcast.15, bf16[256,1024]{1,0:T(8,128)(2,1)} %refs_3_.4, bf16[256,1024]{1,0:T(8,128)(2,1)} %refs_4_.4), custom_call_target="tpu_custom_call" | custom-call | tf_op jit(solution)/shard_map/pallas_call | solution.py:317
  4.4 12.2 %all-to-all-start = ((bf16[64,24,512]{2,1,0:T(8,128)(2,1)}), bf16[64,24,512]{2,1,0:T(8,128)(2,1)S(1)}, u32[]{:S(2)}, u32[]{:S(2)}) async-start(bf16[64,24,512]{2,1,0:T(8,128)(2,1)} %bitcast.14), calls=%async_computation | async-start | bytes 3145728 | tf_op jit(solution)/shard_map/all_to_all | solution.py:345
  17.6 2.4 %collective-permute-start.3 = (bf16[2,1024,128]{2,1,0:T(8,128)(2,1)S(1)}, bf16[2,1024,128]{2,1,0:T(8,128)(2,1)S(1)}, u32[]{:S(2)}, u32[]{:S(2)}) collective-permute-start(bf16[2,1024,128]{2,1,0:T(8,128)(2,1)S(1)} %copy-done.3), channel_id=1, source_target_pairs={{0,1},{1,2},{2,3},{3,0},{4,5},{5,6},{6,7},{7,4},{8,9},{9,10},{10,1... | collective-permute-start | bytes 1572872 | tf_op jit(solution)/shard_map/ppermute | solution.py:331
  20.0 3.2 %collective-permute-start.6 = (bf16[2,128,1024]{2,1,0:T(8,128)(2,1)S(1)}, bf16[2,128,1024]{2,1,0:T(8,128)(2,1)S(1)}, u32[]{:S(2)}, u32[]{:S(2)}) collective-permute-start(bf16[2,128,1024]{2,1,0:T(8,128)(2,1)S(1)} %copy-done.4), channel_id=1, source_target_pairs={{0,1},{1,2},{2,3},{3,0},{4,5},{5,6},{6,7},{7,4},{8,9},{9,10},{10,1... | collective-permute-start | bytes 1572872 | tf_op jit(solution)/shard_map/ppermute | solution.py:331
  23.2 9.5 %collective-permute-done.1.refs_3_ = bf16[2,1024,128]{2,1,0:T(8,128)(2,1)S(1)} collective-permute-done((bf16[2,1024,128]{2,1,0:T(8,128)(2,1)S(1)}, bf16[2,1024,128]{2,1,0:T(8,128)(2,1)S(1)}, u32[]{:S(2)}, u32[]{:S(2)}) %collective-permute-start.1) | collective-permute-done | bytes 524320 | tf_op jit(solution)/shard_map/ppermute | solution.py:332
  32.9 11.1 %collective-permute-done.7.refs_11_ = bf16[2,128,1024]{2,1,0:T(8,128)(2,1)S(1)} collective-permute-done((bf16[2,128,1024]{2,1,0:T(8,128)(2,1)S(1)}, bf16[2,128,1024]{2,1,0:T(8,128)(2,1)S(1)}, u32[]{:S(2)}, u32[]{:S(2)}) %collective-permute-start.7) | collective-permute-done | bytes 524320 | tf_op jit(solution)/shard_map/ppermute | solution.py:332
  44.0 2.1 %collective-permute-start.8 = (bf16[1,128,1024]{2,1,0:T(8,128)(2,1)S(1)}, bf16[1,128,1024]{2,1,0:T(8,128)(2,1)S(1)}, u32[]{:S(2)}, u32[]{:S(2)}) collective-permute-start(bf16[1,128,1024]{2,1,0:T(8,128)(2,1)S(1)} %slice.24), channel_id=1, source_target_pairs={{0,3},{1,0},{2,1},{3,2},{4,7},{5,4},{6,5},{7,6},{8,11},{9,8},{10,9... | collective-permute-start | bytes 786440 | tf_op jit(solution)/shard_map/ppermute | solution.py:335
  46.1 8.7 %collective-permute-done.refs_2_ = bf16[2,1024,128]{2,1,0:T(8,128)(2,1)S(1)} collective-permute-done((bf16[2,1024,128]{2,1,0:T(8,128)(2,1)S(1)}, bf16[2,1024,128]{2,1,0:T(8,128)(2,1)S(1)}, u32[]{:S(2)}, u32[]{:S(2)}) %collective-permute-start) | collective-permute-done | bytes 524320 | tf_op jit(solution)/shard_map/ppermute | solution.py:331
  54.8 3.6 %collective-permute-start.9 = (bf16[1,128,1024]{2,1,0:T(8,128)(2,1)S(1)}, bf16[1,128,1024]{2,1,0:T(8,128)(2,1)S(1)}, u32[]{:S(2)}, u32[]{:S(2)}) collective-permute-start(bf16[1,128,1024]{2,1,0:T(8,128)(2,1)S(1)} %slice.25), channel_id=1, source_target_pairs={{0,1},{1,2},{2,3},{3,0},{4,5},{5,6},{6,7},{7,4},{8,9},{9,10},{10,1... | collective-permute-start | bytes 786440 | tf_op jit(solution)/shard_map/ppermute | solution.py:336
  58.5 12.8 %collective-permute-done.8.refs_12_ = bf16[1,128,1024]{2,1,0:T(8,128)(2,1)S(1)} collective-permute-done((bf16[1,128,1024]{2,1,0:T(8,128)(2,1)S(1)}, bf16[1,128,1024]{2,1,0:T(8,128)(2,1)S(1)}, u32[]{:S(2)}, u32[]{:S(2)}) %collective-permute-start.8) | collective-permute-done | bytes 262176 | tf_op jit(solution)/shard_map/ppermute | solution.py:335
  73.3 8.9 %shard_map.111 = s16[3584,128]{1,0:T(8,128)(2,1)} custom-call(bf16[1536,512]{1,0:T(8,128)(2,1)} %bitcast.10, bf16[2,1024,128]{2,1,0:T(8,128)(2,1)} %refs_2_.3, bf16[2,1024,128]{2,1,0:T(8,128)(2,1)} %copy-done.13, bf16[2,1024,128]{2,1,0:T(8,128)(2,1)} %copy-done.11, bf16[2,1024,128]{2,1,0:T(8,128)(2,1)} %copy-done.15, bf16[2,1024,128]{2,1,0:T(8,128)(2,1)} %refs_3_.7, ...), custom_call_target="tpu_custom_call" | custom-call | tf_op jit(solution)/shard_map/pallas_call | solution.py:317
  82.2 10.6 %all-to-all-start.1 = ((s16[64,56,128]{2,1,0:T(8,128)(2,1)}), s16[64,56,128]{2,1,0:T(8,128)(2,1)S(1)}, u32[]{:S(2)}, u32[]{:S(2)}) async-start(s16[64,56,128]{2,1,0:T(8,128)(2,1)} %bitcast.12), calls=%async_computation.1 | async-start | bytes 1835008 | tf_op jit(solution)/shard_map/all_to_all | solution.py:372
  94.1 3.2 %collective-permute-start.18 = (bf16[768,512]{1,0:T(8,128)(2,1)}, bf16[768,512]{1,0:T(8,128)(2,1)S(1)}, u32[]{:S(2)}, u32[]{:S(2)}) collective-permute-start(bf16[768,512]{1,0:T(8,128)(2,1)} %bitcast.9), channel_id=1, source_target_pairs={{0,1},{1,2},{2,3},{3,0},{4,5},{5,6},{6,7},{7,4},{8,9},{9,10},{10,1... | collective-permute-start | bytes 2359304 | tf_op jit(solution)/shard_map/ppermute | solution.py:351
  99.3 16.6 %collective-permute-done.16.refs_1_ = bf16[768,512]{1,0:T(8,128)(2,1)S(1)} collective-permute-done((bf16[768,512]{1,0:T(8,128)(2,1)}, bf16[768,512]{1,0:T(8,128)(2,1)S(1)}, u32[]{:S(2)}, u32[]{:S(2)}) %collective-permute-start.16) | collective-permute-done | bytes 786464 | tf_op jit(solution)/shard_map/ppermute | solution.py:352
  115.9 3.2 %collective-permute-start.19 = (bf16[768,512]{1,0:T(8,128)(2,1)S(1)}, bf16[768,512]{1,0:T(8,128)(2,1)}, u32[]{:S(2)}, u32[]{:S(2)}) collective-permute-start(bf16[768,512]{1,0:T(8,128)(2,1)S(1)} %collective-permute-done.18.refs_2_), channel_id=1, source_target_pairs={{0,1},{1,2},{2,3},{3,0},{4,5},{5,6},{6,7},{7,4},{8,9},{9,10},{10,1... | collective-permute-start | bytes 2359304 | tf_op jit(solution)/shard_map/ppermute | solution.py:356
  120.1 3.6 %shard_map.112 = (s16[72,1152]{1,0:T(8,128)(2,1)}, s16[72,1152]{1,0:T(8,128)(2,1)}, s16[72,1152]{1,0:T(8,128)(2,1)}, s16[72,1152]{1,0:T(8,128)(2,1)}) custom-call(s32[1]{0:T(128)} %bitcast.refs_0_, s16[3584,128]{1,0:T(8,128)(2,1)} %bitcast.13, bf16[2,384,256]{2,1,0:T(8,128)(2,1)} %get-tuple-element.23.refs_2_), custom_call_target="tpu_custom_call" | custom-call | tf_op jit(solution)/shard_map/pallas_call | solution.py:317
  123.7 2.5 %collective-permute-start.10 = (s16[72,1152]{1,0:T(8,128)(2,1)}, s16[72,1152]{1,0:T(8,128)(2,1)S(1)}, u32[]{:S(2)}, u32[]{:S(2)}) collective-permute-start(s16[72,1152]{1,0:T(8,128)(2,1)} %get-tuple-element.25), channel_id=1, source_target_pairs={{0,1},{1,2},{2,3},{3,0},{4,5},{5,6},{6,7},{7,4},{8,9},{9,10},{10,1... | collective-permute-start | bytes 497672 | tf_op jit(solution)/shard_map/ppermute | solution.py:386
  126.3 25.4 %collective-permute-done.10.from_left = s16[72,1152]{1,0:T(8,128)(2,1)S(1)} collective-permute-done((s16[72,1152]{1,0:T(8,128)(2,1)}, s16[72,1152]{1,0:T(8,128)(2,1)S(1)}, u32[]{:S(2)}, u32[]{:S(2)}) %collective-permute-start.10) | collective-permute-done | bytes 165920 | tf_op jit(solution)/shard_map/ppermute | solution.py:386
  153.4 5.5 %collective-permute-done.11.from_right = s16[72,1152]{1,0:T(8,128)(2,1)S(1)} collective-permute-done((s16[72,1152]{1,0:T(8,128)(2,1)}, s16[72,1152]{1,0:T(8,128)(2,1)S(1)}, u32[]{:S(2)}, u32[]{:S(2)}) %collective-permute-start.11) | collective-permute-done | bytes 165920 | tf_op jit(solution)/shard_map/ppermute | solution.py:387
  160.8 5.2 %collective-permute-done.12.from_opposite = s16[72,1152]{1,0:T(8,128)(2,1)S(1)} collective-permute-done((s16[72,1152]{1,0:T(8,128)(2,1)}, s16[72,1152]{1,0:T(8,128)(2,1)S(1)}, u32[]{:S(2)}, u32[]{:S(2)}) %collective-permute-start.12) | collective-permute-done | bytes 165920 | tf_op jit(solution)/shard_map/ppermute | solution.py:384
  170.6 7.3 %shard_map.114 = (f32[2,1024,128]{2,1,0:T(8,128)}, f32[2,1024,128]{2,1,0:T(8,128)}, f32[2,128,1024]{2,1,0:T(8,128)}) custom-call(bf16[1536,512]{1,0:T(8,128)(2,1)} %bitcast.11, bf16[768,512]{1,0:T(8,128)(2,1)} %copy-done.8, bf16[768,512]{1,0:T(8,128)(2,1)} %copy-done.9, bf16[2,1024,128]{2,1,0:T(8,128)(2,1)} %refs_2_.3, bf16[2,1024,128]{2,1,0:T(8,128)(2,1)} %refs_3_.7, ...), custom_call_target="tpu_custom_call" | custom-call | tf_op jit(solution)/shard_map/pallas_call | solution.py:317
  177.9 6.2 %shard_map.115 = (f32[2,1024,128]{2,1,0:T(8,128)}, f32[2,1024,128]{2,1,0:T(8,128)}, f32[2,128,1024]{2,1,0:T(8,128)}) custom-call(bf16[768,512]{1,0:T(8,128)(2,1)} %collective-permute-done.20.refs_0_, bf16[768,512]{1,0:T(8,128)(2,1)} %collective-permute-done.21.refs_1_, bf16[2,1024,128]{2,1,0:T(8,128)(2,1)} %refs_2_.3, bf16[2,1024,128]{2,1,0:T(8,128)(2,1)} %refs_3_.7, ...), custom_call_target="tpu_custom_call" | custom-call | tf_op jit(solution)/shard_map/pallas_call | solution.py:317
  185.0 6.2 %shard_map.116 = (f32[2,1024,128]{2,1,0:T(8,128)}, f32[2,1024,128]{2,1,0:T(8,128)}, f32[2,128,1024]{2,1,0:T(8,128)}) custom-call(bf16[768,512]{1,0:T(8,128)(2,1)} %copy-done.10, bf16[768,512]{1,0:T(8,128)(2,1)} %collective-permute-done.19.refs_1_, bf16[2,1024,128]{2,1,0:T(8,128)(2,1)} %refs_2_.3, bf16[2,1024,128]{2,1,0:T(8,128)(2,1)} %refs_3_.7, ...), custom_call_target="tpu_custom_call" | custom-call | tf_op jit(solution)/shard_map/pallas_call | solution.py:317
  192.8 6.4 %collective-permute-done.14 = bf16[64,1024]{1,0:T(8,128)(2,1)S(1)} collective-permute-done((bf16[64,1024]{1,0:T(8,128)(2,1)S(1)}, bf16[64,1024]{1,0:T(8,128)(2,1)S(1)}, u32[]{:S(2)}, u32[]{:S(2)}) %collective-permute-start.14) | collective-permute-done | bytes 131104 | tf_op jit(solution)/shard_map/ppermute | solution.py:398
  (85 shorter events, 18.9 us)
Async XLA Ops:
  4.4 67.8 %all-to-all-start = ((bf16[64,24,512]{2,1,0:T(8,128)(2,1)}), bf16[64,24,512]{2,1,0:T(8,128)(2,1)S(1)}, u32[]{:S(2)}, u32[]{:S(2)}) async-start(bf16[64,24,512]{2,1,0:T(8,128)(2,1)} %bitcast.14), calls=%async_computation | async-start | bytes 3145728 | tf_op jit(solution)/shard_map/all_to_all | solution.py:345
  16.7 16.1 %collective-permute-start.1 = (bf16[2,1024,128]{2,1,0:T(8,128)(2,1)S(1)}, bf16[2,1024,128]{2,1,0:T(8,128)(2,1)S(1)}, u32[]{:S(2)}, u32[]{:S(2)}) collective-permute-start(bf16[2,1024,128]{2,1,0:T(8,128)(2,1)S(1)} %copy-done.2), channel_id=1, source_target_pairs={{0,3},{1,0},{2,1},{3,2},{4,7},{5,4},{6,5},{7,6},{8,11},{9,8},{10,9... | collective-permute-start | bytes 1572872 | tf_op jit(solution)/shard_map/ppermute | solution.py:332
  17.6 15.2 %collective-permute-start.3 = (bf16[2,1024,128]{2,1,0:T(8,128)(2,1)S(1)}, bf16[2,1024,128]{2,1,0:T(8,128)(2,1)S(1)}, u32[]{:S(2)}, u32[]{:S(2)}) collective-permute-start(bf16[2,1024,128]{2,1,0:T(8,128)(2,1)S(1)} %copy-done.3), channel_id=1, source_target_pairs={{0,1},{1,2},{2,3},{3,0},{4,5},{5,6},{6,7},{7,4},{8,9},{9,10},{10,1... | collective-permute-start | bytes 1572872 | tf_op jit(solution)/shard_map/ppermute | solution.py:331
  20.0 24.0 %collective-permute-start.7 = (bf16[2,128,1024]{2,1,0:T(8,128)(2,1)S(1)}, bf16[2,128,1024]{2,1,0:T(8,128)(2,1)S(1)}, u32[]{:S(2)}, u32[]{:S(2)}) collective-permute-start(bf16[2,128,1024]{2,1,0:T(8,128)(2,1)S(1)} %copy-done.4), channel_id=1, source_target_pairs={{0,3},{1,0},{2,1},{3,2},{4,7},{5,4},{6,5},{7,6},{8,11},{9,8},{10,9... | collective-permute-start | bytes 1572872 | tf_op jit(solution)/shard_map/ppermute | solution.py:332
  20.0 24.0 %collective-permute-start.6 = (bf16[2,128,1024]{2,1,0:T(8,128)(2,1)S(1)}, bf16[2,128,1024]{2,1,0:T(8,128)(2,1)S(1)}, u32[]{:S(2)}, u32[]{:S(2)}) collective-permute-start(bf16[2,128,1024]{2,1,0:T(8,128)(2,1)S(1)} %copy-done.4), channel_id=1, source_target_pairs={{0,1},{1,2},{2,3},{3,0},{4,5},{5,6},{6,7},{7,4},{8,9},{9,10},{10,1... | collective-permute-start | bytes 1572872 | tf_op jit(solution)/shard_map/ppermute | solution.py:331
  23.2 31.6 %collective-permute-start = (bf16[2,1024,128]{2,1,0:T(8,128)(2,1)S(1)}, bf16[2,1024,128]{2,1,0:T(8,128)(2,1)S(1)}, u32[]{:S(2)}, u32[]{:S(2)}) collective-permute-start(bf16[2,1024,128]{2,1,0:T(8,128)(2,1)S(1)} %copy-done.2), channel_id=1, source_target_pairs={{0,1},{1,2},{2,3},{3,0},{4,5},{5,6},{6,7},{7,4},{8,9},{9,10},{10,1... | collective-permute-start | bytes 1572872 | tf_op jit(solution)/shard_map/ppermute | solution.py:331
  32.7 25.7 %collective-permute-start.4 = (bf16[2,1024,128]{2,1,0:T(8,128)(2,1)S(1)}, bf16[2,1024,128]{2,1,0:T(8,128)(2,1)S(1)}, u32[]{:S(2)}, u32[]{:S(2)}) collective-permute-start(bf16[2,1024,128]{2,1,0:T(8,128)(2,1)S(1)} %copy-done.3), channel_id=1, source_target_pairs={{0,3},{1,0},{2,1},{3,2},{4,7},{5,4},{6,5},{7,6},{8,11},{9,8},{10,9... | collective-permute-start | bytes 1572872 | tf_op jit(solution)/shard_map/ppermute | solution.py:332
  32.8 38.5 %collective-permute-start.2 = (bf16[2,1024,128]{2,1,0:T(8,128)(2,1)S(1)}, bf16[2,1024,128]{2,1,0:T(8,128)(2,1)S(1)}, u32[]{:S(2)}, u32[]{:S(2)}) collective-permute-start(bf16[2,1024,128]{2,1,0:T(8,128)(2,1)S(1)} %collective-permute-done.1.refs_3_), channel_id=1, source_target_pairs={{0,3},{1,0},{2,1},{3,2},{4,7},{5,4},{6,5},{7,6},{8,11},{9,8},{10,9... | collective-permute-start | bytes 1572872 | tf_op jit(solution)/shard_map/ppermute | solution.py:333
  44.0 28.2 %collective-permute-start.5 = (bf16[2,1024,128]{2,1,0:T(8,128)(2,1)S(1)}, bf16[2,1024,128]{2,1,0:T(8,128)(2,1)}, u32[]{:S(2)}, u32[]{:S(2)}) collective-permute-start(bf16[2,1024,128]{2,1,0:T(8,128)(2,1)S(1)} %collective-permute-done.3.refs_6_), channel_id=1, source_target_pairs={{0,1},{1,2},{2,3},{3,0},{4,5},{5,6},{6,7},{7,4},{8,9},{9,10},{10,1... | collective-permute-start | bytes 1572872 | tf_op jit(solution)/shard_map/ppermute | solution.py:334
  44.0 27.2 %collective-permute-start.8 = (bf16[1,128,1024]{2,1,0:T(8,128)(2,1)S(1)}, bf16[1,128,1024]{2,1,0:T(8,128)(2,1)S(1)}, u32[]{:S(2)}, u32[]{:S(2)}) collective-permute-start(bf16[1,128,1024]{2,1,0:T(8,128)(2,1)S(1)} %slice.24), channel_id=1, source_target_pairs={{0,3},{1,0},{2,1},{3,2},{4,7},{5,4},{6,5},{7,6},{8,11},{9,8},{10,9... | collective-permute-start | bytes 786440 | tf_op jit(solution)/shard_map/ppermute | solution.py:335
  54.8 16.4 %collective-permute-start.9 = (bf16[1,128,1024]{2,1,0:T(8,128)(2,1)S(1)}, bf16[1,128,1024]{2,1,0:T(8,128)(2,1)S(1)}, u32[]{:S(2)}, u32[]{:S(2)}) collective-permute-start(bf16[1,128,1024]{2,1,0:T(8,128)(2,1)S(1)} %slice.25), channel_id=1, source_target_pairs={{0,1},{1,2},{2,3},{3,0},{4,5},{5,6},{6,7},{7,4},{8,9},{9,10},{10,1... | collective-permute-start | bytes 786440 | tf_op jit(solution)/shard_map/ppermute | solution.py:336
  82.2 37.0 %all-to-all-start.1 = ((s16[64,56,128]{2,1,0:T(8,128)(2,1)}), s16[64,56,128]{2,1,0:T(8,128)(2,1)S(1)}, u32[]{:S(2)}, u32[]{:S(2)}) async-start(s16[64,56,128]{2,1,0:T(8,128)(2,1)} %bitcast.12), calls=%async_computation.1 | async-start | bytes 1835008 | tf_op jit(solution)/shard_map/all_to_all | solution.py:372
  94.1 21.8 %collective-permute-start.16 = (bf16[768,512]{1,0:T(8,128)(2,1)}, bf16[768,512]{1,0:T(8,128)(2,1)S(1)}, u32[]{:S(2)}, u32[]{:S(2)}) collective-permute-start(bf16[768,512]{1,0:T(8,128)(2,1)} %bitcast.8), channel_id=1, source_target_pairs={{0,3},{1,0},{2,1},{3,2},{4,7},{5,4},{6,5},{7,6},{8,11},{9,8},{10,9... | collective-permute-start | bytes 2359304 | tf_op jit(solution)/shard_map/ppermute | solution.py:352
  94.1 21.8 %collective-permute-start.18 = (bf16[768,512]{1,0:T(8,128)(2,1)}, bf16[768,512]{1,0:T(8,128)(2,1)S(1)}, u32[]{:S(2)}, u32[]{:S(2)}) collective-permute-start(bf16[768,512]{1,0:T(8,128)(2,1)} %bitcast.9), channel_id=1, source_target_pairs={{0,1},{1,2},{2,3},{3,0},{4,5},{5,6},{6,7},{7,4},{8,9},{9,10},{10,1... | collective-permute-start | bytes 2359304 | tf_op jit(solution)/shard_map/ppermute | solution.py:351
  97.3 80.6 %collective-permute-start.21 = (bf16[768,512]{1,0:T(8,128)(2,1)}, bf16[768,512]{1,0:T(8,128)(2,1)}, u32[]{:S(2)}, u32[]{:S(2)}) collective-permute-start(bf16[768,512]{1,0:T(8,128)(2,1)} %bitcast.8), channel_id=1, source_target_pairs={{0,1},{1,2},{2,3},{3,0},{4,5},{5,6},{6,7},{7,4},{8,9},{9,10},{10,1... | collective-permute-start | bytes 2359304 | tf_op jit(solution)/shard_map/ppermute | solution.py:354
  99.0 78.9 %collective-permute-start.20 = (bf16[768,512]{1,0:T(8,128)(2,1)}, bf16[768,512]{1,0:T(8,128)(2,1)}, u32[]{:S(2)}, u32[]{:S(2)}) collective-permute-start(bf16[768,512]{1,0:T(8,128)(2,1)} %bitcast.9), channel_id=1, source_target_pairs={{0,3},{1,0},{2,1},{3,2},{4,7},{5,4},{6,5},{7,6},{8,11},{9,8},{10,9... | collective-permute-start | bytes 2359304 | tf_op jit(solution)/shard_map/ppermute | solution.py:353
  115.9 68.2 %collective-permute-start.17 = (bf16[768,512]{1,0:T(8,128)(2,1)S(1)}, bf16[768,512]{1,0:T(8,128)(2,1)S(1)}, u32[]{:S(2)}, u32[]{:S(2)}) collective-permute-start(bf16[768,512]{1,0:T(8,128)(2,1)S(1)} %collective-permute-done.16.refs_1_), channel_id=1, source_target_pairs={{0,3},{1,0},{2,1},{3,2},{4,7},{5,4},{6,5},{7,6},{8,11},{9,8},{10,9... | collective-permute-start | bytes 2359304 | tf_op jit(solution)/shard_map/ppermute | solution.py:355
  115.9 68.2 %collective-permute-start.19 = (bf16[768,512]{1,0:T(8,128)(2,1)S(1)}, bf16[768,512]{1,0:T(8,128)(2,1)}, u32[]{:S(2)}, u32[]{:S(2)}) collective-permute-start(bf16[768,512]{1,0:T(8,128)(2,1)S(1)} %collective-permute-done.18.refs_2_), channel_id=1, source_target_pairs={{0,1},{1,2},{2,3},{3,0},{4,5},{5,6},{6,7},{7,4},{8,9},{9,10},{10,1... | collective-permute-start | bytes 2359304 | tf_op jit(solution)/shard_map/ppermute | solution.py:356
  123.7 28.0 %collective-permute-start.10 = (s16[72,1152]{1,0:T(8,128)(2,1)}, s16[72,1152]{1,0:T(8,128)(2,1)S(1)}, u32[]{:S(2)}, u32[]{:S(2)}) collective-permute-start(s16[72,1152]{1,0:T(8,128)(2,1)} %get-tuple-element.25), channel_id=1, source_target_pairs={{0,1},{1,2},{2,3},{3,0},{4,5},{5,6},{6,7},{7,4},{8,9},{9,10},{10,1... | collective-permute-start | bytes 497672 | tf_op jit(solution)/shard_map/ppermute | solution.py:386
  151.7 7.2 %collective-permute-start.11 = (s16[72,1152]{1,0:T(8,128)(2,1)}, s16[72,1152]{1,0:T(8,128)(2,1)S(1)}, u32[]{:S(2)}, u32[]{:S(2)}) collective-permute-start(s16[72,1152]{1,0:T(8,128)(2,1)} %get-tuple-element.26), channel_id=1, source_target_pairs={{0,3},{1,0},{2,1},{3,2},{4,7},{5,4},{6,5},{7,6},{8,11},{9,8},{10,9... | collective-permute-start | bytes 497672 | tf_op jit(solution)/shard_map/ppermute | solution.py:387
  158.9 7.1 %collective-permute-start.12 = (s16[72,1152]{1,0:T(8,128)(2,1)}, s16[72,1152]{1,0:T(8,128)(2,1)S(1)}, u32[]{:S(2)}, u32[]{:S(2)}) collective-permute-start(s16[72,1152]{1,0:T(8,128)(2,1)} %get-tuple-element.27), channel_id=1, source_target_pairs={{0,2},{1,3},{2,0},{3,1},{4,6},{5,7},{6,4},{7,5},{8,10},{9,11},{10,... | collective-permute-start | bytes 497672 | tf_op jit(solution)/shard_map/ppermute | solution.py:384
  168.6 24.1 %collective-permute-start.13 = (bf16[64,1024]{1,0:T(8,128)(2,1)}, bf16[64,1024]{1,0:T(8,128)(2,1)S(1)}, u32[]{:S(2)}, u32[]{:S(2)}) collective-permute-start(bf16[64,1024]{1,0:T(8,128)(2,1)} %get-tuple-element.28), channel_id=1, source_target_pairs={{0,1},{1,2},{2,3},{3,0},{4,5},{5,6},{6,7},{7,4},{8,9},{9,10},{10,1... | collective-permute-start | bytes 393224 | tf_op jit(solution)/shard_map/ppermute | solution.py:397
  191.3 8.0 %collective-permute-start.15 = (bf16[64,1024]{1,0:T(8,128)(2,1)S(1)}, bf16[64,1024]{1,0:T(8,128)(2,1)S(1)}, u32[]{:S(2)}, u32[]{:S(2)}) collective-permute-start(bf16[64,1024]{1,0:T(8,128)(2,1)S(1)} %copy-done.22), channel_id=1, source_target_pairs={{0,2},{1,3},{2,0},{3,1},{4,6},{5,7},{6,4},{7,5},{8,10},{9,11},{10,... | collective-permute-start | bytes 393224 | tf_op jit(solution)/shard_map/ppermute | solution.py:395
  191.6 7.6 %collective-permute-start.14 = (bf16[64,1024]{1,0:T(8,128)(2,1)S(1)}, bf16[64,1024]{1,0:T(8,128)(2,1)S(1)}, u32[]{:S(2)}, u32[]{:S(2)}) collective-permute-start(bf16[64,1024]{1,0:T(8,128)(2,1)S(1)} %copy-done.22), channel_id=1, source_target_pairs={{0,3},{1,0},{2,1},{3,2},{4,7},{5,4},{6,5},{7,6},{8,11},{9,8},{10,9... | collective-permute-start | bytes 393224 | tf_op jit(solution)/shard_map/ppermute | solution.py:398
  (23 other events, 356.6 us)
